TPU v7x, 256 devices: a whole 4x4x8 slice. The times are simulated.
256 devices in a mesh: ep: 64 (over z, y, core), tp: 4 (over x).
Axes of the slice: x: 4, y: 4, z: 8, core: 2. Of those that a mesh axis runs over, the one named last changes fastest.
Arguments:
- mixer_input: bfloat16 [32768, 2048], P(('ep', 'tp')), may hold values from -6 to 6
- expert_input: bfloat16 [32768, 2048], P(('ep', 'tp')), may hold values from -6 to 6
- mixer_gain: float32 [2048], replicated, may hold values from 0.1 to 1.9
- expert_gain: float32 [2048], replicated, may hold values from 0.1 to 1.9
- query_weight: bfloat16 [2048, 1024], P(None, 'tp'), may hold values from -0.125 to 0.125
- key_weight: bfloat16 [2048, 1024], P(None, 'tp'), may hold values from -0.125 to 0.125
- value_weight: bfloat16 [2048, 1024], P(None, 'tp'), may hold values from -0.125 to 0.125
- out_weight: bfloat16 [1024, 2048], P('tp'), may hold values from -0.1875 to 0.1875
- decay_rate: float32 [8], P('tp'), may hold values from 0 to 0.12
- routing: int32 [32768, 4], P('ep'), may hold values from 0 to 63, all different within a row; in each aligned block of 128 rows (0 to 127, 128 to 255, ...) at most 12 rows name the same one
- route_weight: float32 [32768, 4], P('ep'), may hold values from 0.2 to 1
- gate_weight: bfloat16 [64, 2048, 1024], P('ep', None, 'tp'), may hold values from -0.125 to 0.125
- up_weight: bfloat16 [64, 2048, 1024], P('ep', None, 'tp'), may hold values from -0.125 to 0.125
- down_weight: bfloat16 [64, 1024, 2048], P('ep', None, 'tp'), may hold values from -0.1875 to 0.1875
- shared_gate: bfloat16 [2048, 512], P(None, 'tp'), may hold values from -0.125 to 0.125
- shared_up: bfloat16 [2048, 512], P(None, 'tp'), may hold values from -0.125 to 0.125
- shared_down: bfloat16 [512, 2048], P(None, 'tp'), may hold values from -0.25 to 0.25
Outputs:
- mixer_output: float32 [32768, 2048], P(('ep', 'tp'))
- expert_output: float32 [32768, 2048], P('ep', 'tp')
Inputs may be any that keep to these rules, and one draw needn't show every extreme that they name: `routing`: each row names 4 different experts. In each aligned block of 128 rows, no expert is named by more than 12 rows, and in some blocks one expert is named by exactly 12 rows.
All inputs are finite; a program needn't handle non-finite values.
Results may differ from a plain program's by a relative error of at most 0.0095.
Values may be sent and summed in bfloat16 or wider, within the bound.
A program may use at most 128 MiB of HBM per device.

v0:
```python
import jax
import jax.numpy as jnp
from jax import lax
from jax.sharding import Mesh
from jax.sharding import PartitionSpec as P

HD = 128
BLK = 64
EP = ("ep_0", "ep_1", "ep_2")
EP_TP = ("ep_0", "ep_1", "ep_2", "tp")
NORM_EPS = 1e-06
ROPE_BASE = 10000.0
EXACT_MATMUL = lax.Precision.HIGHEST


def nothing_yet(value, identity):
    return jax.tree.map(
        lambda a, e: jnp.broadcast_to(jnp.asarray(e, a.dtype), a.shape), value, identity
    )


def entering_2(value, axes, combine, identity):
    before = start = nothing_yet(value, identity)
    subtotal = value
    for axis in reversed(axes):
        count, mine = (lax.axis_size(axis), lax.axis_index(axis))
        pieces = jax.tree.map(lambda part: lax.all_gather(part, axis), subtotal)
        inside, subtotal = (start, start)
        for k in range(count):
            passed = k < mine
            subtotal = combine(subtotal, jax.tree.map(lambda part: part[k], pieces))
            inside = jax.tree.map(lambda new, old: jnp.where(passed, new, old), subtotal, inside)
        before = combine(inside, before)
    return before


def sent_together(arrays, axis, dim, along):
    ends, at = ([], 0)
    for a in arrays[:-1]:
        at += a.shape[along]
        ends.append(at)
    both = jnp.concatenate(arrays, axis=along)
    return tuple(jnp.split(lax.all_gather(both, axis, axis=dim, tiled=True), ends, axis=along))


def norm_rows(inputs, gain_vector):
    values = inputs.astype(jnp.float32)
    scaled = values * lax.rsqrt(jnp.mean(values * values, axis=-1, keepdims=True) + NORM_EPS)
    return (scaled * gain_vector).astype(jnp.bfloat16)


def rotate(head_rows, positions):
    head_size = head_rows.shape[-1]
    inverse = ROPE_BASE ** (-jnp.arange(0, head_size, 2, dtype=jnp.float32) / head_size)
    angles = positions[:, None] * inverse[None, :]
    cosine = jnp.cos(angles)[:, None, :]
    sine_part = jnp.sin(angles)[:, None, :]
    front_half = head_rows[..., : head_size // 2]
    behind = head_rows[..., head_size // 2 :]
    return jnp.concatenate(
        [front_half * cosine - behind * sine_part, front_half * sine_part + behind * cosine],
        axis=-1,
    )


def project(inputs, weight, head_total):
    product = jnp.dot(inputs, weight, preferred_element_type=jnp.float32).astype(jnp.bfloat16)
    product = lax.optimization_barrier(product)
    return product.astype(jnp.float32).reshape(inputs.shape[0], head_total, -1)


def chain_combine(earlier, latter):
    return (earlier[0] * latter[0], latter[0][:, None, None] * earlier[1] + latter[1])


def retain_local(query_heads, key_heads, value_heads, decay_rates):
    length, head_total, head_size = query_heads.shape
    blocks = length // BLK
    log_gamma = -decay_rates
    inner_pos = jnp.arange(BLK, dtype=jnp.float32)
    offsets = inner_pos[:, None] - inner_pos[None, :]
    inside_block_output = jnp.where(
        offsets >= 0, jnp.exp(log_gamma[:, None, None] * jnp.maximum(offsets, 0.0)), 0.0
    )
    key_scale = jnp.exp(log_gamma[None, :] * (BLK - 1.0 - inner_pos)[:, None])
    query_scale = jnp.exp(log_gamma[None, :] * (inner_pos + 1.0)[:, None])
    blocked = (blocks, BLK, head_total, head_size)
    q_blocks = query_heads.reshape(blocked)
    k_blocks = key_heads.reshape(blocked)
    v_blocks = value_heads.reshape(blocked)
    attention_scores = (
        jnp.einsum("nchd,nmhd->nhcm", q_blocks, k_blocks, precision=EXACT_MATMUL)
        * inside_block_output[None]
    )
    nearby = jnp.einsum("nhcm,nmhe->nche", attention_scores, v_blocks, precision=EXACT_MATMUL)
    block_states = jnp.einsum(
        "nchd,nche->nhde", k_blocks * key_scale[None, :, :, None], v_blocks, precision=EXACT_MATMUL
    )
    block_offset_rows = jnp.arange(blocks, dtype=jnp.float32)
    to_end = jnp.exp(log_gamma[None, :] * BLK * (blocks - 1.0 - block_offset_rows)[:, None])
    summary = jnp.einsum("nh,nhde->hde", to_end, block_states, precision=EXACT_MATMUL)
    through = jnp.exp(log_gamma * (BLK * blocks))
    incoming = entering_2(
        (through, summary), EP, chain_combine, (jnp.ones_like(through), jnp.zeros_like(summary))
    )[1]
    block_gaps = block_offset_rows[:, None] - 1.0 - block_offset_rows[None, :]
    carry_mix = jnp.where(
        block_gaps >= 0, jnp.exp(log_gamma[:, None, None] * BLK * jnp.maximum(block_gaps, 0.0)), 0.0
    )
    entering = jnp.einsum("hbj,jhde->bhde", carry_mix, block_states, precision=EXACT_MATMUL)
    entering = (
        entering
        + jnp.exp(log_gamma[None, :] * BLK * block_offset_rows[:, None])[:, :, None, None]
        * incoming[None]
    )
    distant = jnp.einsum(
        "bchd,bhde->bche",
        q_blocks * query_scale[None, :, :, None],
        entering,
        precision=EXACT_MATMUL,
    )
    retained = (nearby + distant).reshape(length, head_total, head_size)
    normed = retained * lax.rsqrt(jnp.mean(retained * retained, axis=-1, keepdims=True) + NORM_EPS)
    return normed.astype(jnp.bfloat16).reshape(length, head_total * head_size)


def assign_slots(routes, source_rows, capacity, expert_count):
    token_count, pick_count = routes.shape
    chosen = routes.reshape(token_count * pick_count)
    onehot = (chosen[:, None] == jnp.arange(expert_count, dtype=jnp.int32)[None, :]).astype(
        jnp.int32
    )
    per_source = onehot.reshape(token_count // source_rows, source_rows * pick_count, expert_count)
    earlier_hits = jnp.cumsum(per_source, axis=1) - per_source
    ranks = jnp.sum(earlier_hits * per_source, axis=2).reshape(token_count * pick_count)
    sources = jnp.arange(token_count * pick_count, dtype=jnp.int32) // (source_rows * pick_count)
    return (chosen, sources * capacity + ranks)


def gather_slots(token_rows, chosen, slot_ids, slot_count, expert_count, pick_count):
    owners = jnp.arange(chosen.shape[0], dtype=jnp.int32) // pick_count + 1
    owner_table = jnp.zeros((slot_count, expert_count), jnp.int32).at[slot_ids, chosen].set(owners)
    padded = jnp.concatenate(
        [jnp.zeros((1, token_rows.shape[1]), token_rows.dtype), token_rows], axis=0
    )
    return padded[owner_table]


def expert_hidden(routed_rows, gate_weight, up_weight):
    per_device = gate_weight.shape[0]
    grouped = routed_rows.reshape(
        routed_rows.shape[0], routed_rows.shape[1] // per_device, per_device, routed_rows.shape[2]
    )
    gate_part = jnp.einsum(
        "snxd,xdf->snxf", grouped, gate_weight, preferred_element_type=jnp.float32
    )
    up_part = jnp.einsum("snxd,xdf->snxf", grouped, up_weight, preferred_element_type=jnp.float32)
    return (jax.nn.silu(gate_part) * up_part).astype(jnp.bfloat16)


def shards(
    mixer_input,
    expert_input,
    mixer_gain,
    expert_gain,
    query_weight,
    key_weight,
    value_weight,
    out_weight,
    decay_rate,
    routing,
    route_weight,
    gate_weight,
    up_weight,
    down_weight,
    shared_gate,
    shared_up,
    shared_down,
):
    own_count = mixer_input.shape[0]
    tp_index = lax.axis_index("tp")
    own_expert_rows = norm_rows(expert_input, expert_gain)
    mixer_rows, expert_rows = sent_together(
        (norm_rows(mixer_input, mixer_gain), own_expert_rows), "tp", 0, 1
    )
    group_count = mixer_rows.shape[0]
    head_total = decay_rate.shape[0]
    positions = (
        lax.axis_index(EP) * group_count + jnp.arange(group_count, dtype=jnp.int32)
    ).astype(jnp.float32)
    query_heads = rotate(project(mixer_rows, query_weight, head_total), positions) * HD ** (-0.5)
    key_heads = rotate(project(mixer_rows, key_weight, head_total), positions)
    value_heads = project(mixer_rows, value_weight, head_total)
    mixed_heads = retain_local(query_heads, key_heads, value_heads, decay_rate)
    mixer_output = lax.psum_scatter(
        jnp.dot(mixed_heads, out_weight, preferred_element_type=jnp.float32).astype(jnp.bfloat16),
        "tp",
        scatter_dimension=0,
        tiled=True,
    ).astype(jnp.float32)
    expert_count = lax.axis_size(EP) * gate_weight.shape[0]
    pick_count = routing.shape[1]
    capacity = (3 * own_count * pick_count + 2 * expert_count - 1) // (2 * expert_count)
    chosen, slot_ids = assign_slots(routing, own_count, capacity, expert_count)
    own_span = own_count * pick_count
    own_chosen = lax.dynamic_slice_in_dim(chosen, tp_index * own_span, own_span, 0)
    own_slots = (
        lax.dynamic_slice_in_dim(slot_ids, tp_index * own_span, own_span, 0) - tp_index * capacity
    )
    outgoing = gather_slots(
        own_expert_rows, own_chosen, own_slots, capacity, expert_count, pick_count
    )
    arrived = lax.all_to_all(outgoing, EP, split_axis=1, concat_axis=1, tiled=True)
    hidden = expert_hidden(
        lax.all_gather(arrived, "tp", axis=0, tiled=True), gate_weight, up_weight
    )
    shared_hidden = (
        jax.nn.silu(jnp.dot(expert_rows, shared_gate, preferred_element_type=jnp.float32))
        * jnp.dot(expert_rows, shared_up, preferred_element_type=jnp.float32)
    ).astype(jnp.bfloat16)
    full_hidden, full_shared = (
        lax.all_gather(hidden, "tp", axis=3, tiled=True),
        lax.all_gather(shared_hidden, "tp", axis=1, tiled=True),
    )
    results = jnp.einsum(
        "snxf,xfe->snxe", full_hidden, down_weight, preferred_element_type=jnp.float32
    ).astype(jnp.bfloat16)
    results = results.reshape(results.shape[0], expert_count, results.shape[3])
    returned = lax.all_to_all(results, EP, split_axis=1, concat_axis=1, tiled=True)
    flat_results = returned.reshape(returned.shape[0] * expert_count, returned.shape[2])
    picked = flat_results[slot_ids * expert_count + chosen].astype(jnp.float32)
    weighted = jnp.sum(
        picked.reshape(group_count, pick_count, -1) * route_weight[:, :, None], axis=1
    )
    shared_result = jnp.dot(full_shared, shared_down, preferred_element_type=jnp.float32)
    expert_output = weighted + shared_result
    return (mixer_output, expert_output)


def solution(mesh):
    finer = Mesh(mesh.devices.reshape(8, 4, 2, mesh.shape["tp"]), ("ep_0", "ep_1", "ep_2", "tp"))
    placed = (
        P(EP_TP, None),
        P(EP_TP, None),
        P(),
        P(),
        P(None, "tp"),
        P(None, "tp"),
        P(None, "tp"),
        P("tp", None),
        P("tp"),
        P(EP, None),
        P(EP, None),
        P(EP, None, "tp"),
        P(EP, None, "tp"),
        P(EP, None, "tp"),
        P(None, "tp"),
        P(None, "tp"),
        P(None, "tp"),
    )
    return jax.shard_map(
        shards,
        mesh=finer,
        in_specs=placed,
        out_specs=(P(EP_TP, None), P(EP, "tp")),
        check_vma=False,
    )
```

profile of v0, /device:TPU:8, one launch (start us, length us, event | category | flops | bytes accessed | tf_op | source)
XLA Modules:
  0.0 539.4 jit_solution(6858122981832166352)
XLA Ops:
  7.2 0.9 copy.108
  8.7 1.2 fusion.36
  9.9 1.2 fusion.39
  11.3 4.8 reduce-window.6
  16.0 0.5 slice_reduce_fusion
  17.0 25.4 %scatter_fusion = s32[12,64]{1,0:T(8,128)S(1)} fusion(s32[12,64]{1,0:T(8,128)S(1)} %broadcast.456, s32[512]{0:T(512)S(1)} %bitcast.156, s32[512]{0:T(512)S(1)} %fusion.96), kind=kCustom, calls=%fused_computation.2 | custom fusion | bytes 10240 | tf_op jit(solution)/shard_map/scatter | solution.py:142
  42.5 1.0 fusion.38
  43.6 4.3 gather_fusion
  47.9 3.7 copy.112
  51.5 108.1 %all_to_all.10 = bf16[12,64,2048]{2,0,1:T(8,128)(2,1)S(1)} all-to-all(bf16[12,64,2048]{2,0,1:T(8,128)(2,1)S(1)} %copy.112), channel_id=1, replica_groups=mesh['ep_0'=8,'ep_1'=4,'ep_2'=2,'tp'=4] {'ep_0','ep_1','ep_2'}, dimensions={1} | all-to-all | bytes 6291456 | tf_op jit(solution)/shard_map/all_to_all | solution.py:213
  159.6 3.4 copy.113
  163.0 1.0 copy-done.9
  164.0 1.0 pad_maximum_fusion
  165.6 114.8 %all-gather.13.cloned.1.call-done = bf16[48,64,2048]{2,1,0:T(8,128)(2,1)} async-done(((bf16[12,64,2048]{2,1,0:T(8,128)(2,1)}), bf16[48,64,2048]{2,1,0:T(8,128)(2,1)}) %all-gather.13.cloned.1.call-update) | async-done | bytes 12582928 | tf_op jit(solution)/shard_map/all_gather | solution.py:215
  280.4 7.9 %fusion.43 = f32[48,64,256]{2,1,0:T(8,128)S(1)} fusion(bf16[48,64,2048]{2,1,0:T(8,128)(2,1)} %all-gather.13.cloned.1.call-done, bf16[1,2048,256]{2,1,0:T(8,128)(2,1)} %param.29), kind=kOutput, calls=%fused_computation.48 | convolution fusion | flops 3221225472 | bytes 16777216 | tf_op jit(solution)/shard_map/snxd,xdf->snxf/dot_general | solution.py:157
  288.3 0.6 copy-done.31
  288.9 5.2 fusion.2
  294.2 0.6 dynamic-slice
  295.5 2.4 all-reduce.1
  298.0 0.6 dynamic-slice.1
  299.4 8.6 %all-reduce.2 = f32[8]{0:T(128)S(1)} all-reduce(f32[8]{0:T(128)S(1)} %get-tuple-element.36), channel_id=4, replica_groups=mesh['ep_0'=8,'ep_1'=4,'ep_2'=2,'tp'=4] {'ep_1'}, use_global_device_ids=true, to_apply=%add.2 | all-reduce | flops 8 | bytes 64
  308.0 0.7 multiply_bitcast_fusion
  308.7 16.6 %all-gather.3 = f32[8,1,2]{2,1,0:T(1,128)S(1)} all-gather(f32[1,1,2]{2,1,0:T(1,128)S(1)} %get-tuple-element.28), channel_id=1, replica_groups=mesh['ep_0'=8,'ep_1'=4,'ep_2'=2,'tp'=4] {'ep_0'}, dimensions={0}, use_global_device_ids=true | all-gather | bytes 72 | tf_op jit(solution)/shard_map/all_gather | solution.py:27
  325.4 0.7 multiply_exponential_fusion.1
  326.1 0.6 exponential_multiply_fusion
  326.7 0.6 slice_bitcast_fusion.8
  327.4 1.7 multiply_cosine_fusion
  329.1 5.5 %all-gather.9.cloned.1.call-done = bf16[512,4096]{1,0:T(8,128)(2,1)} async-done(((bf16[128,4096]{1,0:T(8,128)(2,1)}), bf16[512,4096]{1,0:T(8,128)(2,1)}) %all-gather.9.cloned.1.call-update) | async-done | bytes 4194320 | tf_op jit(solution)/shard_map/all_gather | solution.py:43
  334.6 2.6 fusion.24
  337.5 2.6 fusion.27
  340.3 2.6 fusion.21
  343.0 0.6 fusion.112
  343.6 0.6 fusion.111
  344.2 1.2 multiply_subtract_fusion.1
  345.6 1.1 fusion.54
  346.7 1.5 fusion.47
  348.2 2.2 all-gather.1
  350.4 0.7 copy-done.4
  351.2 12.8 %all_gather.47 = f32[4,2,128,128]{3,2,1,0:T(8,128)S(1)} all-gather(f32[1,2,128,128]{3,2,1,0:T(8,128)S(1)} %fusion.72), channel_id=1, replica_groups=mesh['ep_0'=8,'ep_1'=4,'ep_2'=2,'tp'=4] {'ep_1'}, dimensions={0}, use_global_device_ids=true | all-gather | bytes 655360 | tf_op jit(solution)/shard_map/all_gather | solution.py:27
  364.0 0.8 slice_add_fusion.8
  364.9 43.6 %all-gather.15.cloned.1.call-done = bf16[48,64,1,1024]{3,1,0,2:T(8,128)(2,1)} async-done(((bf16[48,64,1,256]{3,1,0,2:T(8,128)(2,1)}), bf16[48,64,1,1024]{3,1,0,2:T(8,128)(2,1)}) %all-gather.15.cloned.1.call-update) | async-done | bytes 6291472 | tf_op jit(solution)/shard_map/all_gather | solution.py:222
  408.5 6.4 %fusion.6 = bf16[48,64,512]{2,1,0:T(8,128)(2,1)S(1)} fusion(bf16[48,64,1,1024]{3,1,0,2:T(8,128)(2,1)} %all-gather.15.cloned.1.call-done, bf16[1,1024,512]{2,1,0:T(8,128)(2,1)S(1)} %copy-done), kind=kOutput, calls=%fused_computation.14 | convolution fusion | flops 3222798336 | bytes 10485760 | tf_op jit(solution)/shard_map/snxf,xfe->snxe/dot_general | solution.py:225
  414.9 3.4 copy.114
  418.3 10.9 %all-to-all-start.1 = ((bf16[48,64,512]{2,0,1:T(8,128)(2,1)}), bf16[48,64,512]{2,0,1:T(8,128)(2,1)}, u32[]{:S(2)}, u32[]{:S(2)}) async-start(bf16[48,64,512]{2,0,1:T(8,128)(2,1)} %copy.114), calls=%async_computation.2 | async-start | bytes 6291456 | tf_op jit(solution)/shard_map/all_to_all | solution.py:229
  429.4 0.6 fusion.90
  430.0 2.3 convolution_multiply_fusion
  432.3 2.2 fusion.66
  434.5 24.3 %all-gather.11.cloned.1.call-done = f32[8,2,128,128]{3,2,1,0:T(8,128)} async-done(((f32[1,2,128,128]{3,2,1,0:T(8,128)}), f32[8,2,128,128]{3,2,1,0:T(8,128)}) %all-gather.11.cloned.1.call-update) | async-done | bytes 1048592 | tf_op jit(solution)/shard_map/all_gather | solution.py:27
  458.9 1.8 fusion.71
  460.7 1.6 fusion.19
  462.4 1.3 multiply_reduce_fusion.1
  464.3 0.6 mul.685
  465.0 3.4 convolution_convert_fusion
  468.8 2.3 fusion.11
  471.1 2.3 fusion.33
  473.4 18.1 %all_gather.51 = bf16[512,512]{1,0:T(8,128)(2,1)} all-gather(bf16[512,128]{1,0:T(8,128)(2,1)S(1)} %fusion.33), channel_id=1, replica_groups=mesh['ep_0'=8,'ep_1'=4,'ep_2'=2,'tp'=4] {'tp'}, dimensions={1}, use_global_device_ids=true | all-gather | bytes 655360 | tf_op jit(solution)/shard_map/all_gather | solution.py:223
  491.5 12.0 %reduce-scatter.2.cloned.1.call-done = bf16[128,2048]{1,0:T(8,128)(2,1)} async-done(((bf16[512,2048]{1,0:T(8,128)(2,1)}), bf16[128,2048]{1,0:T(8,128)(2,1)}) %reduce-scatter.2.cloned.1.call-update) | async-done | bytes 524304 | tf_op jit(solution)/shard_map/reduce_scatter | solution.py:195
  503.5 2.1 convert_element_type.78
  505.6 2.4 all-to-all-done.1
  508.1 5.3 copy.115
  513.4 9.9 %gather_fusion.1 = bf16[2048,512]{1,0:T(8,128)(2,1)S(1)} fusion(bf16[3072,512]{1,0:T(8,128)(2,1)} %bitcast.155, s32[2048]{0:T(1024)S(1)} %broadcast_clamp_fusion), kind=kCustom, calls=%fused_computation.1 | custom fusion | bytes 4202496 | tf_op jit(solution)/shard_map/gather | solution.py:231
  523.3 3.0 reshape.473
  526.3 4.9 multiply_reduce_fusion
  531.2 1.4 convolution_add_fusion
  (126 shorter events, 4.5 us)
Async XLA Ops:
  7.2 401.3 %copy-start = (bf16[1,1024,512]{2,1,0:T(8,128)(2,1)S(1)}, bf16[1,1024,512]{2,1,0:T(8,128)(2,1)}, u32[]{:S(2)}) copy-start(bf16[1,1024,512]{2,1,0:T(8,128)(2,1)} %param.30) | copy-start | bytes 3145732
  7.2 273.3 %all-gather.13.cloned.1.call-start = ((), (), s32[]{:S(2)}) async-start(), calls=%async_computation.6 | async-start | bytes 15728640 | tf_op jit(solution)/shard_map/all_gather | solution.py:215
  11.2 31.2 %copy-start.6 = (bf16[128,2048]{1,0:T(8,128)(2,1)S(1)}, bf16[128,2048]{1,0:T(8,128)(2,1)}, u32[]{:S(2)}) copy-start(bf16[128,2048]{1,0:T(8,128)(2,1)} %param.17) | copy-start | bytes 1572868
  11.2 31.2 %copy-start.12 = (f32[2048]{0:T(1024)S(1)}, f32[2048]{0:T(1024)}, u32[]{:S(2)}) copy-start(f32[2048]{0:T(1024)} %param.19) | copy-start | bytes 24580
  11.2 31.2 %copy-start.13 = (f32[2048]{0:T(1024)S(1)}, f32[2048]{0:T(1024)}, u32[]{:S(2)}) copy-start(f32[2048]{0:T(1024)} %param.20) | copy-start | bytes 24580
  16.0 26.4 %copy-start.7 = (bf16[128,2048]{1,0:T(8,128)(2,1)S(1)}, bf16[128,2048]{1,0:T(8,128)(2,1)}, u32[]{:S(2)}) copy-start(bf16[128,2048]{1,0:T(8,128)(2,1)} %param.18) | copy-start | bytes 1572868
  163.0 1.0 copy-start.9
  163.0 171.6 %all-gather.9.cloned.1.call-start = ((), (), s32[]{:S(2)}) async-start(), calls=%async_computation.3 | async-start | bytes 5242880 | tf_op jit(solution)/shard_map/all_gather | solution.py:43
  165.1 123.3 %copy-start.32 = (bf16[1,2048,256]{2,1,0:T(8,128)(2,1)S(1)}, bf16[1,2048,256]{2,1,0:T(8,128)(2,1)}, u32[]{:S(2)}) copy-start(bf16[1,2048,256]{2,1,0:T(8,128)(2,1)} %param.28) | copy-start | bytes 3145732
  165.1 243.4 %all-gather.15.cloned.1.call-start = ((), (), s32[]{:S(2)}) async-start(), calls=%async_computation.7 | async-start | bytes 7864320 | tf_op jit(solution)/shard_map/all_gather | solution.py:222
  280.4 8.5 %copy-start.31 = (bf16[48,64,2048]{2,1,0:T(8,128)(2,1)S(1)}, bf16[48,64,2048]{2,1,0:T(8,128)(2,1)}, u32[]{:S(2)}) copy-start(bf16[48,64,2048]{2,1,0:T(8,128)(2,1)} %all-gather.13.cloned.1.call-done) | copy-start | bytes 37748740
  288.9 5.2 copy-start.36
  288.9 6.5 %copy-start.28 = (f32[2]{0:T(128)S(1)}, f32[2]{0:T(128)}, u32[]{:S(2)}) copy-start(f32[2]{0:T(128)} %param.25) | copy-start | bytes 28
  288.9 9.1 %copy-start.35 = (u32[256]{0:T(256)S(1)}, u32[256]{0:T(256)}, u32[]{:S(2)}) copy-start(u32[256]{0:T(256)} %constant.162) | copy-start | bytes 3076
  294.1 164.7 %all-gather.11.cloned.1.call-start = ((), (), s32[]{:S(2)}) async-start(), calls=%async_computation.4 | async-start | bytes 1179648 | tf_op jit(solution)/shard_map/all_gather | solution.py:27
  295.5 41.7 %copy-start.15 = (f32[2]{0:T(128)}, f32[2]{0:T(128)S(1)}, u32[]{:S(2)}) copy-start(f32[2]{0:T(128)S(1)} %get-tuple-element.39) | copy-start | bytes 28
  325.3 11.9 %copy-start.29 = (f32[8]{0:T(128)}, f32[8]{0:T(128)S(1)}, u32[]{:S(2)}) copy-start(f32[8]{0:T(128)S(1)} %iota_add_fusion.2) | copy-start | bytes 100
  343.0 2.7 copy-start.3
  343.0 1.2 copy-start.10
  350.4 0.7 copy-start.4
  418.3 11.0 %copy-start.30 = (f32[8]{0:T(128)S(1)}, f32[8]{0:T(128)}, u32[]{:S(2)}) copy-start(f32[8]{0:T(128)} %copy-done.29) | copy-start | bytes 100
  418.3 89.7 %all-to-all-start.1 = ((bf16[48,64,512]{2,0,1:T(8,128)(2,1)}), bf16[48,64,512]{2,0,1:T(8,128)(2,1)}, u32[]{:S(2)}, u32[]{:S(2)}) async-start(bf16[48,64,512]{2,0,1:T(8,128)(2,1)} %copy.114), calls=%async_computation.2 | async-start | bytes 6291456 | tf_op jit(solution)/shard_map/all_to_all | solution.py:229
  429.2 29.6 %copy-start.19 = (f32[2]{0:T(128)S(1)}, f32[2]{0:T(128)}, u32[]{:S(2)}) copy-start(f32[2]{0:T(128)} %get-tuple-element.31) | copy-start | bytes 28
  429.2 29.6 %copy-start.20 = (f32[2]{0:T(128)S(1)}, f32[2]{0:T(128)}, u32[]{:S(2)}) copy-start(f32[2]{0:T(128)} %get-tuple-element.32) | copy-start | bytes 28
  429.2 29.6 %copy-start.21 = (f32[2]{0:T(128)S(1)}, f32[2]{0:T(128)}, u32[]{:S(2)}) copy-start(f32[2]{0:T(128)} %get-tuple-element.14) | copy-start | bytes 28
  429.2 29.6 %copy-start.22 = (f32[2]{0:T(128)S(1)}, f32[2]{0:T(128)}, u32[]{:S(2)}) copy-start(f32[2]{0:T(128)} %get-tuple-element.15) | copy-start | bytes 28
  429.2 29.6 %copy-start.23 = (f32[2]{0:T(128)S(1)}, f32[2]{0:T(128)}, u32[]{:S(2)}) copy-start(f32[2]{0:T(128)} %get-tuple-element.16) | copy-start | bytes 28
  429.3 29.6 %copy-start.24 = (f32[2]{0:T(128)S(1)}, f32[2]{0:T(128)}, u32[]{:S(2)}) copy-start(f32[2]{0:T(128)} %get-tuple-element.17) | copy-start | bytes 28
  429.3 29.6 %copy-start.25 = (f32[2]{0:T(128)S(1)}, f32[2]{0:T(128)}, u32[]{:S(2)}) copy-start(f32[2]{0:T(128)} %get-tuple-element.18) | copy-start | bytes 28
  429.3 29.6 %copy-start.26 = (f32[2]{0:T(128)S(1)}, f32[2]{0:T(128)}, u32[]{:S(2)}) copy-start(f32[2]{0:T(128)} %get-tuple-element.19) | copy-start | bytes 28
  429.3 31.4 %copy-start.16 = (f32[2]{0:T(128)S(1)}, f32[2]{0:T(128)}, u32[]{:S(2)}) copy-start(f32[2]{0:T(128)} %copy-done.15) | copy-start | bytes 28
  429.3 31.4 %copy-start.18 = (f32[8,2]{0,1:T(2,128)S(1)}, f32[8,2]{0,1:T(2,128)}, u32[]{:S(2)}) copy-start(f32[8,2]{0,1:T(2,128)} %get-tuple-element.26) | copy-start | bytes 196
  429.3 74.2 %reduce-scatter.2.cloned.1.call-start = ((), (), s32[]{:S(2)}) async-start(), calls=%async_computation.5 | async-start | bytes 2621440 | tf_op jit(solution)/shard_map/reduce_scatter | solution.py:195
  432.3 28.4 %copy-start.27 = (pred[8,8]{1,0:T(8,128)(4,1)S(1)}, pred[8,8]{1,0:T(8,128)(4,1)}, u32[]{:S(2)}) copy-start(pred[8,8]{1,0:T(8,128)(4,1)} %fusion.90) | copy-start | bytes 196
  432.3 30.1 %copy-start.1 = (f32[512,2,64]{2,0,1:T(8,128)S(1)}, f32[512,2,64]{2,0,1:T(8,128)}, u32[]{:S(2)}) copy-start(f32[512,2,64]{2,0,1:T(8,128)} %get-tuple-element.4) | copy-start | bytes 786436
  432.3 30.1 %copy-start.17 = (f32[64,2]{0,1:T(2,128)S(1)}, f32[64,2]{0,1:T(2,128)}, u32[]{:S(2)}) copy-start(f32[64,2]{0,1:T(2,128)} %get-tuple-element.24) | copy-start | bytes 1540
  458.8 3.6 copy-start.2
  458.9 3.6 copy-start.8
  464.9 3.6 copy-start.14
  464.9 3.9 copy-start.33
  468.4 2.7 copy-start.34
  526.3 4.9 copy-start.5
  526.3 4.9 copy-start.11
Sparse Core Ops, SparseCore 0:
  163.1 117.2 all-gather.12
  282.8 51.7 all-gather.8
  336.4 72.0 all-gather.14
  410.1 48.6 all-gather.10
  468.5 34.9 reduce-scatter.1
where the time goes:
time: 547 us; the launch traced here: 539 us
  waiting for transfers between devices  203 us (37%)
  blocking collectives  169 us (31%)
  local copies, waits for them, and re-layouts  67.4 us (12%)
  matrix products  46.5 us (9%)
  other arithmetic  26.2 us (5%)
  between operations  16.1 us (3%)
  starting transfers between devices  11.5 us (2%)
    all_gather x1, waiting for transfers between devices, shards(): lax.all_gather(arrived, 'tp', axis=0, tiled=True)  115 us
    all_to_all x1, blocking collectives, shards(): lax.all_to_all(outgoing, EP, split_axis=1, concat_axis=1, tiled=True)  108 us
    all_gather x1, waiting for transfers between devices, shards(): lax.all_gather(hidden, 'tp', axis=3, tiled=True)  43.6 us
    all_gather x3, blocking collectives, entering_2(): pieces = jax.tree.map(lambda part: lax.all_gather(part, axis), subtotal)  31.6 us
    scatter x1, local copies, waits for them, and re-layouts, gather_slots(): jnp.zeros((slot_count, expert_count), jnp.int32).at[slot_ids, chosen]  25.4 us
    all_gather x1, waiting for transfers between devices, entering_2(): pieces = jax.tree.map(lambda part: lax.all_gather(part, axis), subtotal)  24.3 us
    all_gather x1, blocking collectives, shards(): lax.all_gather(shared_hidden, 'tp', axis=1, tiled=True)  18.1 us
    reduce_scatter x1, waiting for transfers between devices, shards(): lax.psum_scatter(jnp.dot(mixed_heads, out_weight, preferred_element_type=...  12 us
  transfers between devices with their start and end apart: 6, of which 6 were waited for; matrix products, arithmetic and copies ran while one was open for 12% of the time, Pallas kernels for 0%

commit v1 on v0

--- a/solution.py
+++ b/solution.py
@@ -219,7 +219,10 @@
         * jnp.dot(expert_rows, shared_up, preferred_element_type=jnp.float32)
     ).astype(jnp.bfloat16)
     full_hidden, full_shared = (
-        lax.all_gather(hidden, "tp", axis=3, tiled=True),
+        jnp.concatenate(
+            lax.all_to_all(jnp.stack([hidden for _ in range(lax.psum(1, "tp"))]), "tp", 0, 0),
+            axis=3,
+        ),
         lax.all_gather(shared_hidden, "tp", axis=1, tiled=True),
     )
     results = jnp.einsum(

time: 547 us -> 558 us (1.020)
  local copies, waits for them, and re-layouts: 67.4 us -> 93.4 us
  waiting for transfers between devices: 203 us -> 182 us
    all_gather x1 -> x0, waiting for transfers between devices: 43.6 us -> none  [shards(): lax.all_gather(hidden, 'tp', axis=3, tiled=True)]
    all_gather x1, waiting for transfers between devices: 5.5 us -> 40.6 us  [sent_together(): lax.all_gather(both, axis, axis=dim, tiled=True)]
    all_gather x1, waiting for transfers between devices: 24.3 us -> 0.01 us  [entering_2(): pieces = jax.tree.map(lambda part: lax.all_gather(part, axis), subtotal)]
    all_to_all x1, waiting for transfers between devices: 2.43 us -> 20.1 us  [shards(): lax.all_to_all(results, EP, split_axis=1, concat_axis=1, tiled=True)]
    all_gather x1, waiting for transfers between devices: 115 us -> 100 us  [shards(): lax.all_gather(arrived, 'tp', axis=0, tiled=True)]
    another operation x2 -> x4, local copies, waits for them, and re-layouts: 0.01 us -> 14.5 us
    reshape x0 -> x1, local copies, waits for them, and re-layouts: none -> 11.6 us  [shards(): jnp.concatenate(lax.all_to_all(jnp.stack([hidden for _ in range(lax.psum(...]
    all_to_all x0 -> x1, waiting for transfers between devices: none -> 8.64 us  [shards(): lax.all_to_all(jnp.stack([hidden for _ in range(lax.psum(1, 'tp'))]), 'tp...]
  transfers between devices with their start and end apart: 6 -> 6, of which waited for: 6 -> 5; matrix products, arithmetic and copies ran while one was open for 12% -> 17% of each run, Pallas kernels for 0% -> 0%
where the time goes in v1:
time: 558 us; the launch traced here: 551 us
  waiting for transfers between devices  182 us (33%)
  blocking collectives  170 us (30%)
  local copies, waits for them, and re-layouts  93.4 us (17%)
  matrix products  45.5 us (8%)
  other arithmetic  26.3 us (5%)
  starting transfers between devices  16.6 us (3%)
  between operations  16.4 us (3%)
    all_to_all x1, blocking collectives, shards(): lax.all_to_all(outgoing, EP, split_axis=1, concat_axis=1, tiled=True)  108 us
    all_gather x1, waiting for transfers between devices, shards(): lax.all_gather(arrived, 'tp', axis=0, tiled=True)  100 us
    all_gather x1, waiting for transfers between devices, sent_together(): lax.all_gather(both, axis, axis=dim, tiled=True)  40.6 us
    all_gather x3, blocking collectives, entering_2(): pieces = jax.tree.map(lambda part: lax.all_gather(part, axis), subtotal)  31.8 us
    scatter x1, local copies, waits for them, and re-layouts, gather_slots(): jnp.zeros((slot_count, expert_count), jnp.int32).at[slot_ids, chosen]  25.4 us
    all_to_all x1, waiting for transfers between devices, shards(): lax.all_to_all(results, EP, split_axis=1, concat_axis=1, tiled=True)  20.1 us
    all_gather x1, blocking collectives, shards(): lax.all_gather(shared_hidden, 'tp', axis=1, tiled=True)  18.6 us
    reduce_scatter x1, waiting for transfers between devices, shards(): lax.psum_scatter(jnp.dot(mixed_heads, out_weight, preferred_element_type=...  12.7 us
  transfers between devices with their start and end apart: 6, of which 5 were waited for; matrix products, arithmetic and copies ran while one was open for 17% of the time, Pallas kernels for 0%

profile of v1, /device:TPU:8, one launch (start us, length us, event | category | flops | bytes accessed | tf_op | source)
XLA Modules:
  0.0 550.5 jit_solution(14182518665546374406)
XLA Ops:
  7.2 0.9 copy.110
  8.7 1.2 fusion.32
  9.9 1.2 fusion.35
  11.3 4.8 reduce-window.6
  17.0 25.4 %scatter_fusion = s32[12,64]{1,0:T(8,128)S(1)} fusion(s32[12,64]{1,0:T(8,128)S(1)} %broadcast.459, s32[512]{0:T(512)S(1)} %bitcast.161, s32[512]{0:T(512)S(1)} %fusion.92), kind=kCustom, calls=%fused_computation.2 | custom fusion | bytes 10240 | tf_op jit(solution)/shard_map/scatter | solution.py:142
  42.5 1.0 fusion.34
  43.6 4.3 gather_fusion
  47.8 3.7 copy.114
  51.5 108.1 %all_to_all.15 = bf16[12,64,2048]{2,0,1:T(8,128)(2,1)S(1)} all-to-all(bf16[12,64,2048]{2,0,1:T(8,128)(2,1)S(1)} %copy.114), channel_id=1, replica_groups=mesh['ep_0'=8,'ep_1'=4,'ep_2'=2,'tp'=4] {'ep_0','ep_1','ep_2'}, dimensions={1} | all-to-all | bytes 6291456 | tf_op jit(solution)/shard_map/all_to_all | solution.py:213
  159.6 3.4 copy.115
  163.0 1.0 copy-done.9
  164.0 1.0 pad_maximum_fusion
  165.1 0.6 dynamic-slice
  166.4 2.4 all-reduce.1
  170.3 9.1 %all-reduce.2 = f32[8]{0:T(128)S(1)} all-reduce(f32[8]{0:T(128)S(1)} %get-tuple-element.36), channel_id=4, replica_groups=mesh['ep_0'=8,'ep_1'=4,'ep_2'=2,'tp'=4] {'ep_1'}, use_global_device_ids=true, to_apply=%add.2 | all-reduce | flops 8 | bytes 64
  179.5 0.7 multiply_bitcast_fusion
  180.2 100.2 %all-gather.12.cloned.1.call-done = bf16[48,64,2048]{2,1,0:T(8,128)(2,1)} async-done(((bf16[12,64,2048]{2,1,0:T(8,128)(2,1)}), bf16[48,64,2048]{2,1,0:T(8,128)(2,1)}) %all-gather.12.cloned.1.call-update) | async-done | bytes 12582928 | tf_op jit(solution)/shard_map/all_gather | solution.py:215
  280.4 7.9 %fusion.39 = f32[48,64,256]{2,1,0:T(8,128)S(1)} fusion(bf16[48,64,2048]{2,1,0:T(8,128)(2,1)} %all-gather.12.cloned.1.call-done, bf16[1,2048,256]{2,1,0:T(8,128)(2,1)} %param.29), kind=kOutput, calls=%fused_computation.47 | convolution fusion | flops 3221225472 | bytes 16777216 | tf_op jit(solution)/shard_map/snxd,xdf->snxf/dot_general | solution.py:157
  288.9 4.1 fusion.14
  293.0 3.5 stack.2
  296.5 5.4 all-to-all-start.1
  301.9 16.8 %all-gather.3 = f32[8,1,2]{2,1,0:T(1,128)S(1)} all-gather(f32[1,1,2]{2,1,0:T(1,128)S(1)} %get-tuple-element.28), channel_id=1, replica_groups=mesh['ep_0'=8,'ep_1'=4,'ep_2'=2,'tp'=4] {'ep_0'}, dimensions={0}, use_global_device_ids=true | all-gather | bytes 72 | tf_op jit(solution)/shard_map/all_gather | solution.py:27
  318.7 0.7 multiply_exponential_fusion.1
  319.4 0.7 exponential_multiply_fusion
  320.0 0.6 slice_bitcast_fusion.8
  320.7 1.7 multiply_cosine_fusion
  322.5 40.6 %all-gather.8.cloned.1.call-done = bf16[512,4096]{1,0:T(8,128)(2,1)} async-done(((bf16[128,4096]{1,0:T(8,128)(2,1)}), bf16[512,4096]{1,0:T(8,128)(2,1)}) %all-gather.8.cloned.1.call-update) | async-done | bytes 4194320 | tf_op jit(solution)/shard_map/all_gather | solution.py:43
  363.1 2.6 fusion.20
  365.9 2.6 fusion.23
  368.7 2.6 fusion.17
  371.4 0.6 fusion.108
  372.0 0.6 fusion.107
  372.6 1.2 multiply_subtract_fusion.1
  374.0 1.1 fusion.50
  375.1 1.5 fusion.43
  376.6 2.0 all-gather.1
  378.6 0.7 copy-done.4
  379.4 13.0 %all_gather.44 = f32[4,2,128,128]{3,2,1,0:T(8,128)S(1)} all-gather(f32[1,2,128,128]{3,2,1,0:T(8,128)S(1)} %fusion.68), channel_id=1, replica_groups=mesh['ep_0'=8,'ep_1'=4,'ep_2'=2,'tp'=4] {'ep_1'}, dimensions={0}, use_global_device_ids=true | all-gather | bytes 655360 | tf_op jit(solution)/shard_map/all_gather | solution.py:27
  392.4 0.7 slice_add_fusion.8
  393.4 8.6 %all-to-all-done.1 = bf16[4,48,64,1,256]{4,2,1,3,0:T(8,128)(2,1)} async-done(((bf16[4,48,64,1,256]{4,2,1,3,0:T(8,128)(2,1)}), bf16[4,48,64,1,256]{4,2,1,3,0:T(8,128)(2,1)}, u32[]{:S(2)}, u32[]{:S(2)}) %all-to-all-start.1) | async-done | bytes 6291488 | tf_op jit(solution)/shard_map/all_to_all | solution.py:223
  402.0 11.6 %copy.116 = bf16[48,64,1,4,256]{4,3,1,0,2:T(4,128)(2,1)} copy(bf16[48,64,1,4,256]{4,1,0,2,3:T(8,128)(2,1)} %bitcast.44) | data formatting | bytes 12582912 | tf_op jit(solution)/shard_map/reshape | solution.py:222
  413.6 11.0 %reshape.473 = bf16[48,64,1024]{2,1,0:T(8,128)(2,1)} reshape(bf16[48,64,1,4,256]{4,3,1,0,2:T(4,128)(2,1)} %copy.116) | data formatting | bytes 12582912 | tf_op jit(solution)/shard_map/reshape.11
  424.5 6.4 %convolution_convert_fusion.1 = bf16[48,64,512]{2,1,0:T(8,128)(2,1)S(1)} fusion(bf16[48,64,1024]{2,1,0:T(8,128)(2,1)} %reshape.473, bf16[1,1024,512]{2,1,0:T(8,128)(2,1)S(1)} %copy-done), kind=kOutput, calls=%fused_computation.12 | convolution fusion | flops 3222798336 | bytes 10485760 | tf_op jit(solution)/shard_map/snxf,xfe->snxe/dot_general | solution.py:228
  431.0 3.4 copy.117
  434.4 10.8 %all-to-all-start.2 = ((bf16[48,64,512]{2,0,1:T(8,128)(2,1)}), bf16[48,64,512]{2,0,1:T(8,128)(2,1)}, u32[]{:S(2)}, u32[]{:S(2)}) async-start(bf16[48,64,512]{2,0,1:T(8,128)(2,1)} %copy.117), calls=%async_computation.3 | async-start | bytes 6291456 | tf_op jit(solution)/shard_map/all_to_all | solution.py:232
  445.7 0.6 fusion.86
  446.4 2.2 convolution_multiply_fusion
  448.6 2.2 fusion.62
  450.9 1.8 fusion.67
  452.7 1.6 fusion.15
  454.4 1.3 multiply_reduce_fusion.1
  456.3 0.6 mul.685
  457.0 3.4 convolution_convert_fusion
  460.8 2.3 fusion.6
  463.1 2.3 fusion.29
  465.5 18.6 %all_gather.47 = bf16[512,512]{1,0:T(8,128)(2,1)} all-gather(bf16[512,128]{1,0:T(8,128)(2,1)S(1)} %fusion.29), channel_id=1, replica_groups=mesh['ep_0'=8,'ep_1'=4,'ep_2'=2,'tp'=4] {'tp'}, dimensions={1}, use_global_device_ids=true | all-gather | bytes 655360 | tf_op jit(solution)/shard_map/all_gather | solution.py:226
  484.0 12.7 %reduce-scatter.2.cloned.1.call-done = bf16[128,2048]{1,0:T(8,128)(2,1)} async-done(((bf16[512,2048]{1,0:T(8,128)(2,1)}), bf16[128,2048]{1,0:T(8,128)(2,1)}) %reduce-scatter.2.cloned.1.call-update) | async-done | bytes 524304 | tf_op jit(solution)/shard_map/reduce_scatter | solution.py:195
  496.7 2.1 convert_element_type.80
  498.8 20.1 %all-to-all-done.2 = bf16[48,64,512]{2,0,1:T(8,128)(2,1)} async-done(((bf16[48,64,512]{2,0,1:T(8,128)(2,1)}), bf16[48,64,512]{2,0,1:T(8,128)(2,1)}, u32[]{:S(2)}, u32[]{:S(2)}) %all-to-all-start.2) | async-done | bytes 3145760 | tf_op jit(solution)/shard_map/all_to_all | solution.py:232
  518.9 5.3 copy.118
  524.3 9.9 %gather_fusion.1 = bf16[2048,512]{1,0:T(8,128)(2,1)S(1)} fusion(bf16[3072,512]{1,0:T(8,128)(2,1)} %bitcast.160, s32[2048]{0:T(1024)S(1)} %broadcast_clamp_fusion), kind=kCustom, calls=%fused_computation.1 | custom fusion | bytes 4202496 | tf_op jit(solution)/shard_map/gather | solution.py:234
  534.2 3.0 reshape.482
  537.2 4.9 multiply_reduce_fusion
  542.1 1.4 convolution_add_fusion
  (128 shorter events, 5.9 us)
Async XLA Ops:
  7.2 417.4 %copy-start = (bf16[1,1024,512]{2,1,0:T(8,128)(2,1)S(1)}, bf16[1,1024,512]{2,1,0:T(8,128)(2,1)}, u32[]{:S(2)}) copy-start(bf16[1,1024,512]{2,1,0:T(8,128)(2,1)} %param.30) | copy-start | bytes 3145732
  7.2 273.2 %all-gather.12.cloned.1.call-start = ((), (), s32[]{:S(2)}) async-start(), calls=%async_computation.7 | async-start | bytes 15728640 | tf_op jit(solution)/shard_map/all_gather | solution.py:215
  11.2 31.2 %copy-start.6 = (bf16[128,2048]{1,0:T(8,128)(2,1)S(1)}, bf16[128,2048]{1,0:T(8,128)(2,1)}, u32[]{:S(2)}) copy-start(bf16[128,2048]{1,0:T(8,128)(2,1)} %param.17) | copy-start | bytes 1572868
  11.2 31.2 %copy-start.12 = (f32[2048]{0:T(1024)S(1)}, f32[2048]{0:T(1024)}, u32[]{:S(2)}) copy-start(f32[2048]{0:T(1024)} %param.19) | copy-start | bytes 24580
  11.2 31.2 %copy-start.13 = (f32[2048]{0:T(1024)S(1)}, f32[2048]{0:T(1024)}, u32[]{:S(2)}) copy-start(f32[2048]{0:T(1024)} %param.20) | copy-start | bytes 24580
  16.0 26.4 %copy-start.7 = (bf16[128,2048]{1,0:T(8,128)(2,1)S(1)}, bf16[128,2048]{1,0:T(8,128)(2,1)}, u32[]{:S(2)}) copy-start(bf16[128,2048]{1,0:T(8,128)(2,1)} %param.18) | copy-start | bytes 1572868
  162.9 1.0 copy-start.9
  162.9 2.1 copy-start.36
  162.9 3.4 copy-start.28
  162.9 5.9 %copy-start.35 = (u32[256]{0:T(256)S(1)}, u32[256]{0:T(256)}, u32[]{:S(2)}) copy-start(u32[256]{0:T(256)} %constant.162) | copy-start | bytes 3076
  163.0 200.1 %all-gather.8.cloned.1.call-start = ((), (), s32[]{:S(2)}) async-start(), calls=%async_computation.4 | async-start | bytes 5242880 | tf_op jit(solution)/shard_map/all_gather | solution.py:43
  166.4 152.3 %copy-start.15 = (f32[2]{0:T(128)}, f32[2]{0:T(128)S(1)}, u32[]{:S(2)}) copy-start(f32[2]{0:T(128)S(1)} %get-tuple-element.39) | copy-start | bytes 28
  179.4 141.3 %copy-start.29 = (f32[8]{0:T(128)}, f32[8]{0:T(128)S(1)}, u32[]{:S(2)}) copy-start(f32[8]{0:T(128)S(1)} %iota_add_fusion.2) | copy-start | bytes 100
  180.2 108.1 %copy-start.32 = (bf16[1,2048,256]{2,1,0:T(8,128)(2,1)S(1)}, bf16[1,2048,256]{2,1,0:T(8,128)(2,1)}, u32[]{:S(2)}) copy-start(bf16[1,2048,256]{2,1,0:T(8,128)(2,1)} %param.28) | copy-start | bytes 3145732
  280.4 8.5 %copy-start.31 = (bf16[48,64,2048]{2,1,0:T(8,128)(2,1)S(1)}, bf16[48,64,2048]{2,1,0:T(8,128)(2,1)}, u32[]{:S(2)}) copy-start(bf16[48,64,2048]{2,1,0:T(8,128)(2,1)} %all-gather.12.cloned.1.call-done) | copy-start | bytes 37748740
  296.5 105.5 %all-to-all-start.1 = ((bf16[4,48,64,1,256]{4,2,1,3,0:T(8,128)(2,1)}), bf16[4,48,64,1,256]{4,2,1,3,0:T(8,128)(2,1)}, u32[]{:S(2)}, u32[]{:S(2)}) async-start(bf16[4,48,64,1,256]{4,2,1,3,0:T(8,128)(2,1)} %stack.2), calls=%async_computation.2 | async-start | bytes 12582912 | tf_op jit(solution)/shard_map/all_to_all | solution.py:223
  301.9 149.0 %all-gather.10.cloned.1.call-start = ((), (), s32[]{:S(2)}) async-start(), calls=%async_computation.5 | async-start | bytes 1179648 | tf_op jit(solution)/shard_map/all_gather | solution.py:27
  371.4 2.7 copy-start.3
  371.4 1.2 copy-start.10
  378.6 0.7 copy-start.4
  434.4 11.3 %copy-start.30 = (f32[8]{0:T(128)S(1)}, f32[8]{0:T(128)}, u32[]{:S(2)}) copy-start(f32[8]{0:T(128)} %copy-done.29) | copy-start | bytes 100
  434.4 84.5 %all-to-all-start.2 = ((bf16[48,64,512]{2,0,1:T(8,128)(2,1)}), bf16[48,64,512]{2,0,1:T(8,128)(2,1)}, u32[]{:S(2)}, u32[]{:S(2)}) async-start(bf16[48,64,512]{2,0,1:T(8,128)(2,1)} %copy.117), calls=%async_computation.3 | async-start | bytes 6291456 | tf_op jit(solution)/shard_map/all_to_all | solution.py:232
  445.3 5.6 %copy-start.19 = (f32[2]{0:T(128)S(1)}, f32[2]{0:T(128)}, u32[]{:S(2)}) copy-start(f32[2]{0:T(128)} %get-tuple-element.31) | copy-start | bytes 28
  445.3 5.6 %copy-start.20 = (f32[2]{0:T(128)S(1)}, f32[2]{0:T(128)}, u32[]{:S(2)}) copy-start(f32[2]{0:T(128)} %get-tuple-element.32) | copy-start | bytes 28
  445.3 5.6 %copy-start.21 = (f32[2]{0:T(128)S(1)}, f32[2]{0:T(128)}, u32[]{:S(2)}) copy-start(f32[2]{0:T(128)} %get-tuple-element.14) | copy-start | bytes 28
  445.3 5.6 %copy-start.22 = (f32[2]{0:T(128)S(1)}, f32[2]{0:T(128)}, u32[]{:S(2)}) copy-start(f32[2]{0:T(128)} %get-tuple-element.15) | copy-start | bytes 28
  445.3 5.6 %copy-start.23 = (f32[2]{0:T(128)S(1)}, f32[2]{0:T(128)}, u32[]{:S(2)}) copy-start(f32[2]{0:T(128)} %get-tuple-element.16) | copy-start | bytes 28
  445.3 5.6 %copy-start.24 = (f32[2]{0:T(128)S(1)}, f32[2]{0:T(128)}, u32[]{:S(2)}) copy-start(f32[2]{0:T(128)} %get-tuple-element.17) | copy-start | bytes 28
  445.4 5.6 %copy-start.25 = (f32[2]{0:T(128)S(1)}, f32[2]{0:T(128)}, u32[]{:S(2)}) copy-start(f32[2]{0:T(128)} %get-tuple-element.18) | copy-start | bytes 28
  445.4 5.6 %copy-start.26 = (f32[2]{0:T(128)S(1)}, f32[2]{0:T(128)}, u32[]{:S(2)}) copy-start(f32[2]{0:T(128)} %get-tuple-element.19) | copy-start | bytes 28
  445.4 7.3 %copy-start.16 = (f32[2]{0:T(128)S(1)}, f32[2]{0:T(128)}, u32[]{:S(2)}) copy-start(f32[2]{0:T(128)} %copy-done.15) | copy-start | bytes 28
  445.4 7.3 %copy-start.18 = (f32[8,2]{0,1:T(2,128)S(1)}, f32[8,2]{0,1:T(2,128)}, u32[]{:S(2)}) copy-start(f32[8,2]{0,1:T(2,128)} %get-tuple-element.26) | copy-start | bytes 196
  445.4 51.3 %reduce-scatter.2.cloned.1.call-start = ((), (), s32[]{:S(2)}) async-start(), calls=%async_computation.6 | async-start | bytes 2621440 | tf_op jit(solution)/shard_map/reduce_scatter | solution.py:195
  448.6 4.1 copy-start.27
  448.6 5.8 %copy-start.1 = (f32[512,2,64]{2,0,1:T(8,128)S(1)}, f32[512,2,64]{2,0,1:T(8,128)}, u32[]{:S(2)}) copy-start(f32[512,2,64]{2,0,1:T(8,128)} %get-tuple-element.4) | copy-start | bytes 786436
  448.6 5.8 %copy-start.17 = (f32[64,2]{0,1:T(2,128)S(1)}, f32[64,2]{0,1:T(2,128)}, u32[]{:S(2)}) copy-start(f32[64,2]{0,1:T(2,128)} %get-tuple-element.24) | copy-start | bytes 1540
  450.9 3.6 copy-start.2
  450.9 3.6 copy-start.8
  456.9 3.7 copy-start.14
  457.0 3.9 copy-start.33
  460.4 2.7 copy-start.34
  537.2 4.9 copy-start.5
  537.2 4.9 copy-start.11
Sparse Core Ops, SparseCore 0:
  163.1 117.2 all-gather.11
  282.8 80.2 all-gather.7
  393.3 39.3 all-gather.9
  460.5 36.1 reduce-scatter.1
